TPU v7x, 32 devices: a whole 2x2x4 slice. The times are simulated.
32 devices in a mesh: ep: 8 (over z, x), tp: 4 (over y, core).
Axes of the slice: x: 2, y: 2, z: 4, core: 2. Of those that a mesh axis runs over, the one named last changes fastest.
Arguments:
- tokens: bfloat16 [192, 3072], P('ep'), may hold values from -6 to 6
- norm_gain: float32 [3072], replicated, may hold values from 0.1 to 1.9
- routing: int32 [192, 4], P('ep'), may hold values from 0 to 7, all different within a row; in each aligned block of 24 rows (0 to 23, 24 to 47, ...) at most 13 rows name the same one
- route_weight: float32 [192, 4], P('ep'), may hold values from 0.05 to 1
- w_gate: bfloat16 [8, 3072, 3072], P('ep', None, 'tp'), may hold values from -0.3125 to 0.3125
- w_up: bfloat16 [8, 3072, 3072], P('ep', None, 'tp'), may hold values from -0.3125 to 0.3125
- w_down: bfloat16 [8, 3072, 3072], P('ep', 'tp'), may hold values from -0.01953125 to 0.01953125
Outputs:
- mixed: bfloat16 [192, 3072], P('ep', 'tp')
Inputs may be any that keep to these rules, and one draw needn't show every extreme that they name: `routing`: each row names 4 different experts. Within the rows of one device (aligned blocks of 24 rows) no expert is named by more than 13 rows, a bound that some block reaches.
All inputs are finite; a program needn't handle non-finite values.
Results may differ from a plain program's by a relative error of at most 0.019.
Values may be sent and summed in bfloat16 or wider, within the bound.
No kernel may reach another device: no remote copies, remote signals or barrier semaphores. Data moves between devices by JAX's collectives and lax.ppermute only.
A program may use at most 64 MiB of HBM per device.

v0:
```python
import jax
import jax.numpy as jnp
from jax import lax
from jax.sharding import PartitionSpec as P

NORM_EPS = 1e-06
CLAMP_LIMIT = 7.0
SIGMOID_SCALE = 1.702


def slot_index(route_rows, expert_total, capacity):
    flat_ids = route_rows.reshape(-1)
    one_hot = (flat_ids[:, None] == jnp.arange(expert_total, dtype=jnp.int32)[None, :]).astype(
        jnp.int32
    )
    before = jnp.cumsum(one_hot, axis=0) - one_hot
    ranked = jnp.sum(before * one_hot, axis=1)
    return flat_ids * capacity + ranked


def local(tokens, norm_gain, routing, route_weight, w_gate, w_up, w_down):
    tok_count = tokens.shape[0]
    width = tokens.shape[1]
    top_count = routing.shape[1]
    expert_total = lax.axis_size("ep") * w_gate.shape[0]
    capacity = max(2, tok_count * top_count // expert_total + 1)
    slice_width = width // lax.axis_size("tp")
    values = tokens.astype(jnp.float32)
    scaled = values * lax.rsqrt(jnp.mean(values * values, axis=-1, keepdims=True) + NORM_EPS)
    normal = (scaled * norm_gain).astype(jnp.bfloat16)
    dest = slot_index(routing, expert_total, capacity)
    slot_ids = jnp.arange(expert_total * capacity, dtype=jnp.int32)
    select = jnp.sum(dest.reshape(1, tok_count, top_count) == slot_ids[:, None, None], axis=2)
    sending = jnp.dot(
        select.astype(jnp.bfloat16), normal, preferred_element_type=jnp.float32
    ).astype(jnp.bfloat16)
    gate_mat = w_gate[0]
    up_mat = w_up[0]
    down_mat = w_down[0]
    own_share = lax.dynamic_slice_in_dim(
        sending, lax.axis_index("tp") * slice_width, slice_width, 1
    )
    arrived = lax.all_to_all(own_share, "ep", split_axis=0, concat_axis=0, tiled=True)
    pieces = lax.all_gather(arrived, "tp", axis=1, tiled=True)
    gate_pre = jnp.dot(pieces, gate_mat, preferred_element_type=jnp.float32)
    up_pre = jnp.dot(pieces, up_mat, preferred_element_type=jnp.float32)
    gated = jnp.minimum(gate_pre, CLAMP_LIMIT)
    upper = jnp.clip(up_pre, -CLAMP_LIMIT, CLAMP_LIMIT)
    hidden = ((upper + 1.0) * gated * jax.nn.sigmoid(SIGMOID_SCALE * gated)).astype(jnp.bfloat16)
    summed = lax.psum_scatter(
        lax.dot_general(
            down_mat, hidden, (((0,), (1,)), ((), ())), preferred_element_type=jnp.float32
        ).astype(jnp.bfloat16),
        "tp",
        scatter_dimension=0,
        tiled=True,
    )
    back = lax.all_to_all(summed, "ep", split_axis=1, concat_axis=1, tiled=True)
    picked = back[:, dest].reshape(slice_width, tok_count, top_count)
    mixed = jnp.sum(picked.astype(jnp.float32) * route_weight[None, :, :], axis=2)
    return mixed.T.astype(jnp.bfloat16)


def solution(mesh):
    placed = (
        P("ep", None),
        P(),
        P("ep", None),
        P("ep", None),
        P("ep", None, "tp"),
        P("ep", None, "tp"),
        P("ep", "tp", None),
    )
    return jax.shard_map(
        local, mesh=mesh, in_specs=placed, out_specs=P("ep", "tp"), check_vma=False
    )
```

profile of v0, /device:TPU:0, one launch (start us, length us, event | category | flops | bytes accessed | tf_op | source)
XLA Modules:
  0.0 87.3 jit_solution(828306079801427838)
XLA Ops:
  6.5 0.8 copy.14
  7.3 0.1 eq.28
  7.4 0.1 fusion.48
  7.5 0.1 reduce_window_sum.11
  7.6 0.2 select_reduce_fusion
  7.8 0.1 reduce_sum.41
  7.9 0.1 copy.16
  8.0 0.1 convert_reduce_fusion
  8.1 1.0 %fusion.37 = f32[24]{0:T(128)S(1)} fusion(bf16[24,3072]{1,0:T(8,128)(2,1)} %param.7), kind=kLoop, calls=%fused_computation.23 | loop fusion | flops 221160 | bytes 147552 | tf_op jit(solution)/shard_map/reduce_sum | solution.py:29
  9.2 1.3 %fusion.44 = bf16[104,3072]{1,0:T(8,128)(2,1)S(1)} fusion(bf16[24,3072]{1,0:T(8,128)(2,1)} %param.7, f32[3072]{0:T(1024)} %param.8, f32[24]{0:T(128)S(1)} %add_rsqrt_fusion, s32[104,24]{0,1:T(8,128)S(1)} %convert_reduce_fusion), kind=kOutput, calls=%fused_computation.32 | convolution fusion | flops 15632832 | bytes 808800 | tf_op jit(solution)/shard_map/dot_general | solution.py:34
  10.6 15.0 %all_to_all.24 = bf16[8,13,768]{2,1,0:T(8,128)(2,1)S(1)} all-to-all(bf16[8,13,768]{2,1,0:T(8,128)(2,1)S(1)} %all_to_all.16), channel_id=1, replica_groups=mesh['ep'=8,'tp'=4] {'ep'}, dimensions={0} | all-to-all | bytes 319488 | tf_op jit(solution)/shard_map/all_to_all | solution.py:43
  25.6 0.1 all_to_all.18
  25.7 7.8 %all_gather.3 = bf16[104,3072]{1,0:T(8,128)(2,1)S(1)} all-gather(bf16[104,768]{1,0:T(8,128)(2,1)S(1)} %all_to_all.18), channel_id=1, replica_groups=mesh['ep'=8,'tp'=4] {'tp'}, dimensions={1}, use_global_device_ids=true | all-gather | bytes 798720 | tf_op jit(solution)/shard_map/all_gather | solution.py:44
  33.5 3.2 %fusion.12 = f32[104,768]{1,0:T(8,128)S(1)} fusion(bf16[104,3072]{1,0:T(8,128)(2,1)S(1)} %all_gather.3, bf16[1,3072,768]{2,1,0:T(8,128)(2,1)} %param.11), kind=kOutput, calls=%fused_computation.9 | convolution fusion | flops 490813440 | bytes 5677056 | tf_op jit(solution)/shard_map/dot_general | solution.py:45
  36.7 6.5 %fusion.9 = bf16[3072,104]{0,1:T(8,128)(2,1)} fusion(bf16[1,768,3072]{2,1,0:T(8,128)(2,1)} %param.13, f32[104,768]{1,0:T(8,128)S(1)} %fusion.12, bf16[104,3072]{1,0:T(8,128)(2,1)S(1)} %all_gather.3, bf16[1,3072,768]{2,1,0:T(8,128)(2,1)} %param.12), kind=kOutput, calls=%fused_computation.8 | convolution fusion | flops 982505472 | bytes 11034624 | tf_op jit(solution)/shard_map/dot_general | solution.py:51
  43.2 0.1 mul.76
  43.4 0.1 copy.17
  43.4 20.2 %reduce-scatter.2.cloned.1.call-done = bf16[768,104]{0,1:T(8,128)(2,1)} async-done(((bf16[3072,104]{0,1:T(8,128)(2,1)}), bf16[768,104]{0,1:T(8,128)(2,1)}) %reduce-scatter.2.cloned.1.call-update) | async-done | bytes 159760 | tf_op jit(solution)/shard_map/reduce_scatter | solution.py:50
  63.7 1.6 %all_to_all.19 = bf16[768,8,13]{0,2,1:T(8,128)(2,1)} reshape(bf16[768,104]{0,1:T(8,128)(2,1)} %reduce-scatter.2.cloned.1.call-done) | data formatting | bytes 319488 | tf_op jit(solution)/shard_map/all_to_all | solution.py:58
  65.3 5.5 %all-to-all-start.1 = ((bf16[768,8,13]{0,2,1:T(8,128)(2,1)}), bf16[768,8,13]{0,2,1:T(8,128)(2,1)S(1)}, u32[]{:S(2)}, u32[]{:S(2)}) async-start(bf16[768,8,13]{0,2,1:T(8,128)(2,1)} %all_to_all.19), calls=%async_computation.2 | async-start | bytes 393216 | tf_op jit(solution)/shard_map/all_to_all | solution.py:58
  70.8 7.8 %all-to-all-done.1 = bf16[768,8,13]{0,2,1:T(8,128)(2,1)S(1)} async-done(((bf16[768,8,13]{0,2,1:T(8,128)(2,1)}), bf16[768,8,13]{0,2,1:T(8,128)(2,1)S(1)}, u32[]{:S(2)}, u32[]{:S(2)}) %all-to-all-start.1) | async-done | bytes 159776 | tf_op jit(solution)/shard_map/all_to_all | solution.py:58
  78.7 0.8 gather_fusion
  79.5 0.1 reshape.54
  79.6 0.9 multiply_reduce_fusion
  (12 shorter events, 0.2 us)
Async XLA Ops:
  6.5 57.1 %reduce-scatter.2.cloned.1.call-start = ((), (), s32[]{:S(2)}) async-start(), calls=%async_computation.3 | async-start | bytes 798720 | tf_op jit(solution)/shard_map/reduce_scatter | solution.py:50
  36.7 6.7 %copy-start = (f32[24,4]{0,1:T(4,128)S(1)}, f32[24,4]{0,1:T(4,128)}, u32[]{:S(2)}) copy-start(f32[24,4]{0,1:T(4,128)} %param.10) | copy-start | bytes 1156
  65.3 13.3 %all-to-all-start.1 = ((bf16[768,8,13]{0,2,1:T(8,128)(2,1)}), bf16[768,8,13]{0,2,1:T(8,128)(2,1)S(1)}, u32[]{:S(2)}, u32[]{:S(2)}) async-start(bf16[768,8,13]{0,2,1:T(8,128)(2,1)} %all_to_all.19), calls=%async_computation.2 | async-start | bytes 393216 | tf_op jit(solution)/shard_map/all_to_all | solution.py:58
Sparse Core Ops, SparseCore 0:
  43.4 20.2 reduce-scatter.1
where the time goes:
time: 87.7 us; the launch traced here: 87.3 us
  waiting for transfers between devices  28 us (32%)
  blocking collectives  22.9 us (26%)
  between operations  13.5 us (15%)
  matrix products  11 us (13%)
  starting transfers between devices  5.5 us (6%)
  local copies, waits for them, and re-layouts  3.96 us (5%)
  other arithmetic  2.44 us (3%)
    reduce_scatter x1, waiting for transfers between devices, local(): lax.psum_scatter(lax.dot_general(down_mat, hidden, (((0,), (1,)), ((), ()...  20.2 us
    all_to_all x1, blocking collectives, local(): lax.all_to_all(own_share, 'ep', split_axis=0, concat_axis=0, tiled=True)  15 us
    all_gather x1, blocking collectives, local(): pieces = lax.all_gather(arrived, 'tp', axis=1, tiled=True)  7.82 us
    all_to_all x1, waiting for transfers between devices, local(): back = lax.all_to_all(summed, 'ep', split_axis=1, concat_axis=1, tiled=True)  7.77 us
    dot_general x1, matrix products, local(): lax.dot_general(down_mat, hidden, (((0,), (1,)), ((), ())), preferred_ele...  6.54 us
    all_to_all x1, starting transfers between devices, local(): back = lax.all_to_all(summed, 'ep', split_axis=1, concat_axis=1, tiled=True)  5.5 us
    dot_general x1, matrix products, local(): gate_pre = jnp.dot(pieces, gate_mat, preferred_element_type=jnp.float32)  3.18 us
  transfers between devices with their start and end apart: 2, of which 2 were waited for; matrix products, arithmetic and copies ran while one was open for 0% of the time, Pallas kernels for 0%

commit v1 on v0

--- a/solution.py
+++ b/solution.py
@@ -55,7 +55,10 @@
         scatter_dimension=0,
         tiled=True,
     )
-    back = lax.all_to_all(summed, "ep", split_axis=1, concat_axis=1, tiled=True)
+    back = jnp.concatenate(
+        lax.all_to_all(jnp.stack(jnp.split(summed, lax.axis_size("ep"), axis=1)), "ep", 0, 0),
+        axis=1,
+    )
     picked = back[:, dest].reshape(slice_width, tok_count, top_count)
     mixed = jnp.sum(picked.astype(jnp.float32) * route_weight[None, :, :], axis=2)
     return mixed.T.astype(jnp.bfloat16)

time: 87.7 us -> 97.5 us (1.11)
  local copies, waits for them, and re-layouts: 3.96 us -> 13.3 us
    unnamed x4 -> x11, local copies, waits for them, and re-layouts: 0.85 us -> 10.5 us
    all_to_all x2 -> x0, local copies, waits for them, and re-layouts: 1.71 us -> none  [local(): back = lax.all_to_all(summed, 'ep', split_axis=1, concat_axis=1, tiled=True)]
    another operation x0 -> x1, local copies, waits for them, and re-layouts: none -> 1.35 us  [local(): jnp.stack(jnp.split(summed, lax.axis_size('ep'), axis=1))]
where the time goes in v1:
time: 97.5 us; the launch traced here: 96.6 us
  waiting for transfers between devices  28 us (29%)
  blocking collectives  22.9 us (23%)
  between operations  13.5 us (14%)
  local copies, waits for them, and re-layouts  13.3 us (14%)
  matrix products  11 us (11%)
  starting transfers between devices  5.5 us (6%)
  other arithmetic  2.44 us (3%)
    reduce_scatter x1, waiting for transfers between devices, local(): lax.psum_scatter(lax.dot_general(down_mat, hidden, (((0,), (1,)), ((), ()...  20.2 us
    all_to_all x1, blocking collectives, local(): lax.all_to_all(own_share, 'ep', split_axis=0, concat_axis=0, tiled=True)  15 us
    unnamed x11, local copies, waits for them, and re-layouts  10.5 us
    all_gather x1, blocking collectives, local(): pieces = lax.all_gather(arrived, 'tp', axis=1, tiled=True)  7.82 us
    all_to_all x1, waiting for transfers between devices, local(): lax.all_to_all(jnp.stack(jnp.split(summed, lax.axis_size('ep'), axis=1)),...  7.77 us
    dot_general x1, matrix products, local(): lax.dot_general(down_mat, hidden, (((0,), (1,)), ((), ())), preferred_ele...  6.54 us
    all_to_all x1, starting transfers between devices, local(): lax.all_to_all(jnp.stack(jnp.split(summed, lax.axis_size('ep'), axis=1)),...  5.5 us
    dot_general x1, matrix products, local(): gate_pre = jnp.dot(pieces, gate_mat, preferred_element_type=jnp.float32)  3.18 us
  transfers between devices with their start and end apart: 2, of which 2 were waited for; matrix products, arithmetic and copies ran while one was open for 0% of the time, Pallas kernels for 0%

profile of v1, /device:TPU:0, one launch (start us, length us, event | category | flops | bytes accessed | tf_op | source)
XLA Modules:
  0.0 96.6 jit_solution(892729293245453577)
XLA Ops:
  6.5 0.8 copy.14
  7.3 0.1 eq.28
  7.5 0.1 reduce_window_sum.11
  7.6 0.2 select_reduce_fusion
  7.8 0.1 reduce_sum.41
  8.1 1.0 %fusion.37 = f32[24]{0:T(128)S(1)} fusion(bf16[24,3072]{1,0:T(8,128)(2,1)} %param.7), kind=kLoop, calls=%fused_computation.23 | loop fusion | flops 221160 | bytes 147552 | tf_op jit(solution)/shard_map/reduce_sum | solution.py:29
  9.2 1.3 %fusion.44 = bf16[104,3072]{1,0:T(8,128)(2,1)S(1)} fusion(bf16[24,3072]{1,0:T(8,128)(2,1)} %param.7, f32[3072]{0:T(1024)} %param.8, f32[24]{0:T(128)S(1)} %add_rsqrt_fusion, s32[104,24]{0,1:T(8,128)S(1)} %convert_reduce_fusion), kind=kOutput, calls=%fused_computation.32 | convolution fusion | flops 15632832 | bytes 808800 | tf_op jit(solution)/shard_map/dot_general | solution.py:34
  10.6 15.0 %all_to_all.17 = bf16[8,13,768]{2,1,0:T(8,128)(2,1)S(1)} all-to-all(bf16[8,13,768]{2,1,0:T(8,128)(2,1)S(1)} %all_to_all.11), channel_id=1, replica_groups=mesh['ep'=8,'tp'=4] {'ep'}, dimensions={0} | all-to-all | bytes 319488 | tf_op jit(solution)/shard_map/all_to_all | solution.py:43
  25.7 7.8 %all_gather.3 = bf16[104,3072]{1,0:T(8,128)(2,1)S(1)} all-gather(bf16[104,768]{1,0:T(8,128)(2,1)S(1)} %all_to_all.13), channel_id=1, replica_groups=mesh['ep'=8,'tp'=4] {'tp'}, dimensions={1}, use_global_device_ids=true | all-gather | bytes 798720 | tf_op jit(solution)/shard_map/all_gather | solution.py:44
  33.5 3.2 %fusion.12 = f32[104,768]{1,0:T(8,128)S(1)} fusion(bf16[104,3072]{1,0:T(8,128)(2,1)S(1)} %all_gather.3, bf16[1,3072,768]{2,1,0:T(8,128)(2,1)} %param.11), kind=kOutput, calls=%fused_computation.9 | convolution fusion | flops 490813440 | bytes 5677056 | tf_op jit(solution)/shard_map/dot_general | solution.py:45
  36.7 6.5 %fusion.9 = bf16[3072,104]{0,1:T(8,128)(2,1)} fusion(bf16[1,768,3072]{2,1,0:T(8,128)(2,1)} %param.13, f32[104,768]{1,0:T(8,128)S(1)} %fusion.12, bf16[104,3072]{1,0:T(8,128)(2,1)S(1)} %all_gather.3, bf16[1,3072,768]{2,1,0:T(8,128)(2,1)} %param.12), kind=kOutput, calls=%fused_computation.8 | convolution fusion | flops 982505472 | bytes 11034624 | tf_op jit(solution)/shard_map/dot_general | solution.py:51
  43.4 20.2 %reduce-scatter.2.cloned.1.call-done = bf16[768,104]{0,1:T(8,128)(2,1)} async-done(((bf16[3072,104]{0,1:T(8,128)(2,1)}), bf16[768,104]{0,1:T(8,128)(2,1)}) %reduce-scatter.2.cloned.1.call-update) | async-done | bytes 159760 | tf_op jit(solution)/shard_map/reduce_scatter | solution.py:50
  63.7 1.3 %fusion.56 = bf16[8,768,13]{1,2,0:T(8,128)(2,1)} fusion(bf16[768,104]{0,1:T(8,128)(2,1)} %reduce-scatter.2.cloned.1.call-done), kind=kLoop, calls=%fused_computation.56 | loop fusion | bytes 44544
  65.0 1.4 %fusion.55 = bf16[8,768,13]{1,2,0:T(8,128)(2,1)} fusion(bf16[8,768,13]{1,2,0:T(8,128)(2,1)} %fusion.56, bf16[768,104]{0,1:T(8,128)(2,1)} %reduce-scatter.2.cloned.1.call-done), kind=kLoop, calls=%fused_computation.54 | loop fusion | bytes 49152
  66.4 1.4 %fusion.54 = bf16[8,768,13]{1,2,0:T(8,128)(2,1)} fusion(bf16[8,768,13]{1,2,0:T(8,128)(2,1)} %fusion.55, bf16[768,104]{0,1:T(8,128)(2,1)} %reduce-scatter.2.cloned.1.call-done), kind=kLoop, calls=%fused_computation.52 | loop fusion | bytes 49152
  67.8 1.4 %fusion.53 = bf16[8,768,13]{1,2,0:T(8,128)(2,1)} fusion(bf16[8,768,13]{1,2,0:T(8,128)(2,1)} %fusion.54, bf16[768,104]{0,1:T(8,128)(2,1)} %reduce-scatter.2.cloned.1.call-done), kind=kLoop, calls=%fused_computation.50 | loop fusion | bytes 49152
  69.1 1.4 %fusion.52 = bf16[8,768,13]{1,2,0:T(8,128)(2,1)} fusion(bf16[8,768,13]{1,2,0:T(8,128)(2,1)} %fusion.53, bf16[768,104]{0,1:T(8,128)(2,1)} %reduce-scatter.2.cloned.1.call-done), kind=kLoop, calls=%fused_computation.48 | loop fusion | bytes 49152
  70.5 1.4 %fusion.51 = bf16[8,768,13]{1,2,0:T(8,128)(2,1)} fusion(bf16[8,768,13]{1,2,0:T(8,128)(2,1)} %fusion.52, bf16[768,104]{0,1:T(8,128)(2,1)} %reduce-scatter.2.cloned.1.call-done), kind=kLoop, calls=%fused_computation.46 | loop fusion | bytes 49152
  71.9 1.4 %fusion.50 = bf16[8,768,13]{1,2,0:T(8,128)(2,1)} fusion(bf16[8,768,13]{1,2,0:T(8,128)(2,1)} %fusion.51, bf16[768,104]{0,1:T(8,128)(2,1)} %reduce-scatter.2.cloned.1.call-done), kind=kLoop, calls=%fused_computation.44 | loop fusion | bytes 49152
  73.3 1.4 %fusion.49 = bf16[8,768,13]{1,2,0:T(8,128)(2,1)} fusion(bf16[8,768,13]{1,2,0:T(8,128)(2,1)} %fusion.50, bf16[768,104]{0,1:T(8,128)(2,1)} %reduce-scatter.2.cloned.1.call-done), kind=kLoop, calls=%fused_computation.42 | loop fusion | bytes 49152 | tf_op jit(solution)/shard_map/stack | solution.py:59
  74.6 5.5 %all-to-all-start.1 = ((bf16[8,768,13]{1,2,0:T(8,128)(2,1)}), bf16[8,768,13]{1,2,0:T(8,128)(2,1)S(1)}, u32[]{:S(2)}, u32[]{:S(2)}) async-start(bf16[8,768,13]{1,2,0:T(8,128)(2,1)} %fusion.49), calls=%async_computation.2 | async-start | bytes 393216 | tf_op jit(solution)/shard_map/all_to_all | solution.py:59
  80.2 7.8 %all-to-all-done.1 = bf16[8,768,13]{1,2,0:T(8,128)(2,1)S(1)} async-done(((bf16[8,768,13]{1,2,0:T(8,128)(2,1)}), bf16[8,768,13]{1,2,0:T(8,128)(2,1)S(1)}, u32[]{:S(2)}, u32[]{:S(2)}) %all-to-all-start.1) | async-done | bytes 159776 | tf_op jit(solution)/shard_map/all_to_all | solution.py:59
  88.0 0.8 gather_fusion
  88.9 0.9 multiply_reduce_fusion
  (19 shorter events, 0.8 us)
Async XLA Ops:
  6.5 57.1 %reduce-scatter.2.cloned.1.call-start = ((), (), s32[]{:S(2)}) async-start(), calls=%async_computation.3 | async-start | bytes 798720 | tf_op jit(solution)/shard_map/reduce_scatter | solution.py:50
  36.7 6.7 %copy-start = (f32[24,4]{0,1:T(4,128)S(1)}, f32[24,4]{0,1:T(4,128)}, u32[]{:S(2)}) copy-start(f32[24,4]{0,1:T(4,128)} %param.10) | copy-start | bytes 1156
  74.6 13.3 %all-to-all-start.1 = ((bf16[8,768,13]{1,2,0:T(8,128)(2,1)}), bf16[8,768,13]{1,2,0:T(8,128)(2,1)S(1)}, u32[]{:S(2)}, u32[]{:S(2)}) async-start(bf16[8,768,13]{1,2,0:T(8,128)(2,1)} %fusion.49), calls=%async_computation.2 | async-start | bytes 393216 | tf_op jit(solution)/shard_map/all_to_all | solution.py:59
Sparse Core Ops, SparseCore 0:
  43.4 20.2 reduce-scatter.1
